TPU v7x, 256 devices: a 4x2x16 block of a 4x16x16 slice. The times are simulated.
256 devices in a mesh: grp: 2 (over y), kv: 16 (over z), tp: 8 (over x, core).
Axes of the slice: x: 4, y: 2, z: 16, core: 2. Of those that a mesh axis runs over, the one named last changes fastest.
The devices are a block of a 4x16x16 slice.
Arguments:
- piece_tokens: bfloat16 [8192, 2048], P(('grp', 'kv')), parts along dimension 0, may hold values from -6 to 6
- dec_tokens: bfloat16 [128, 2048], P(('grp', 'kv')), parts along dimension 0, may hold values from -6 to 6
- norm_gain: float32 [2048], replicated, may hold values from 0.1 to 1.9
- query_weight: bfloat16 [2048, 1024], P(None, 'tp'), may hold values from -0.125 to 0.125
- key_weight: bfloat16 [2048, 1024], P(None, 'tp'), may hold values from -0.125 to 0.125
- value_weight: bfloat16 [2048, 1024], P(None, 'tp'), may hold values from -0.125 to 0.125
- forget_weight: bfloat16 [2048, 8], P(None, 'tp'), may hold values from -0.125 to 0.125
- forget_bias: float32 [8], P('tp'), may hold values from 3 to 13
- out_weight: bfloat16 [1024, 2048], P(None, 'tp'), may hold values from -0.1875 to 0.1875
- cache_keys: bfloat16 [131072, 1024], P(('grp', 'kv'), 'tp'), parts along dimension 0, may hold values from -480 to 480
- cache_values: bfloat16 [131072, 1024], P(('grp', 'kv'), 'tp'), parts along dimension 0, may hold values from -6 to 6
- cache_gates: float32 [8, 131072], P('tp', ('grp', 'kv')), parts along dimension 1, as said below
- dec_keys: bfloat16 [128, 2048, 1024], P(('grp', 'kv'), None, 'tp'), parts along dimension 0, may hold values from -480 to 480
- dec_values: bfloat16 [128, 2048, 1024], P(('grp', 'kv'), None, 'tp'), parts along dimension 0, may hold values from -6 to 6
- dec_gates: float32 [128, 8, 2048], P(('grp', 'kv'), 'tp'), parts along dimension 0, as said below
- dec_lengths: int32 [128], P(('grp', 'kv')), parts along dimension 0, may hold values from 1 to 2048, as said below
Outputs:
- piece_out: bfloat16 [8192, 2048], P(('grp', 'kv'), 'tp'), parts along dimension 0
- dec_out: bfloat16 [128, 2048], P(('grp', 'kv'), 'tp'), parts along dimension 0
- piece_keys: bfloat16 [8192, 1024], P(('grp', 'kv'), 'tp'), parts along dimension 0
- piece_values: bfloat16 [8192, 1024], P(('grp', 'kv'), 'tp'), parts along dimension 0
There are 2 independent parts, one for each index of `grp`. A program takes and returns all parts, laid end to end along the dimension named above; an argument that names none is the same for every part. Nothing has to cross between parts.
Inputs may be any that keep to these rules, and one draw needn't show every extreme that they name: cache_gates never falls along positions and is 0 at the last cached position. dec_gates never falls along a sequence's live slots and is 0 at its last live slot and beyond. Slots 0 to dec_lengths[b] - 1 of sequence b are live; some sequence has exactly 2048.
All inputs are finite; a program needn't handle non-finite values.
Results may differ from a plain program's by a relative error of at most 0.015.
Values may be sent and summed in bfloat16 or wider, within the bound.
A program may use at most 64 MiB of HBM per device.

v0:
```python
import math

import jax
import jax.numpy as jnp
from jax import lax
from jax.sharding import PartitionSpec as P

norm_eps = 1e-05


def from_everyone(shard, axis):
    devices = lax.axis_size(axis)
    return lax.all_to_all(
        jnp.broadcast_to(shard[None], (devices, *shard.shape)), axis, 0, 0, tiled=True
    )


def folded_in_pairs(pieces, combine):
    while len(jax.tree.leaves(pieces)[0]) > 1:
        pieces = jax.vmap(combine)(*(pieces[side::2] for side in (0, 1)))
    return pieces[0]


def prefix(shard, axis, combine, identity):
    devices, mine = (lax.axis_size(axis), lax.axis_index(axis))
    passed = jnp.arange(devices) < mine

    def kept(part, zero, own):
        part = jnp.where(
            passed.reshape(-1, *(1 for _ in own.shape)), part, jnp.asarray(zero, own.dtype)
        )
        return part

    pieces = from_everyone(shard, axis)
    return folded_in_pairs(kept(pieces, identity, shard), combine)


def taken_together(shard, axis):
    everything = from_everyone(shard, axis)
    return jnp.max(everything, axis=0)


def cut_along(shard, dim, devices):
    shape = shard.shape
    parts = shard.reshape(*shape[:dim], devices, shape[dim] // devices, *shape[dim + 1 :])
    return jnp.moveaxis(parts, dim, 0)


def sent_and_summed(shard, axis, dim):
    devices = lax.axis_size(axis)
    parts = lax.all_to_all(cut_along(shard, dim, devices), axis, 0, 0, tiled=True)
    return jnp.sum(parts.astype(jnp.float32), axis=0)


def sent_and_summed_2(shard, axis, dim):
    devices = lax.axis_size(axis)
    parts = lax.all_to_all(cut_along(shard, dim, devices), axis, 0, 0, tiled=True)
    return jnp.sum(parts, axis=0)


def sent_together(arrays, axis, dim, along):
    both = jnp.concatenate(arrays, axis=along)
    result, at, finished = (lax.all_gather(both, axis, axis=dim, tiled=True), 0, [])
    for a in arrays:
        finished.append(lax.slice_in_dim(result, at, at + a.shape[along], axis=along))
        at += a.shape[along]
    return tuple(finished)


def rms_norm(tokens, norm_gain):
    values = tokens.astype(jnp.float32)
    factor = lax.rsqrt(jnp.mean(values * values, axis=-1, keepdims=True) + norm_eps)
    return (values * factor * norm_gain).astype(jnp.bfloat16)


def project(tokens, norm_gain, query_weight, key_weight, value_weight, forget_weight, forget_bias):
    normed = rms_norm(tokens, norm_gain)
    queries = jnp.dot(normed, query_weight, preferred_element_type=jnp.float32).astype(jnp.bfloat16)
    key_rows = jnp.dot(normed, key_weight, preferred_element_type=jnp.float32).astype(jnp.bfloat16)
    value_rows = jnp.dot(normed, value_weight, preferred_element_type=jnp.float32).astype(
        jnp.bfloat16
    )
    log_gates = jax.nn.log_sigmoid(
        jnp.dot(normed, forget_weight, preferred_element_type=jnp.float32) + forget_bias
    )
    return (queries, key_rows, value_rows, log_gates)


def add_pair(earlier_sum, later_sum):
    return earlier_sum + later_sum


def shards(
    piece_tokens,
    dec_tokens,
    norm_gain,
    query_weight,
    key_weight,
    value_weight,
    forget_weight,
    forget_bias,
    out_weight,
    cache_keys,
    cache_values,
    cache_gates,
    dec_keys,
    dec_values,
    dec_gates,
    dec_lengths,
):
    piece_count = piece_tokens.shape[0]
    local_heads = forget_weight.shape[1]
    head_size = query_weight.shape[1] // local_heads
    score_scale = head_size ** (-0.5)
    piece_parts = project(
        piece_tokens, norm_gain, query_weight, key_weight, value_weight, forget_weight, forget_bias
    )
    dec_parts = project(
        dec_tokens, norm_gain, query_weight, key_weight, value_weight, forget_weight, forget_bias
    )
    piece_queries, piece_keys, piece_values, piece_gates = piece_parts
    dec_queries, dec_new_keys, dec_new_values, dec_gate_now = dec_parts
    running = jnp.cumsum(piece_gates, axis=0)
    offset = prefix(running[-1], "kv", add_pair, jnp.zeros_like(running[-1]))
    piece_bias = -(running + offset[None, :]).T
    all_queries = lax.all_gather(piece_queries, "kv", axis=0, tiled=True)
    shard_index = lax.axis_index("kv")
    key_order = shard_index * piece_count + jnp.arange(piece_count, dtype=jnp.int32)
    cache_rows = cache_keys.shape[0]
    cache_key_heads = cache_keys.reshape(cache_rows, local_heads, head_size)
    cache_value_heads = cache_values.reshape(cache_rows, local_heads, head_size)
    piece_key_heads = piece_keys.reshape(piece_count, local_heads, head_size)
    piece_value_heads = piece_values.reshape(piece_count, local_heads, head_size)
    total_rows = all_queries.shape[0]
    block_rows = math.gcd(total_rows, 512)
    block_count = total_rows // block_rows
    query_blocks = all_queries.reshape(block_count, block_rows, local_heads, head_size)
    block_starts = jnp.arange(block_count, dtype=jnp.int32) * block_rows

    def block_terms(inputs):
        query_block, first_row = inputs
        cache_scores = (
            jnp.einsum(
                "qhd,khd->hqk", query_block, cache_key_heads, preferred_element_type=jnp.float32
            )
            * score_scale
            + cache_gates[:, None, :]
        )
        piece_scores = (
            jnp.einsum(
                "qhd,khd->hqk", query_block, piece_key_heads, preferred_element_type=jnp.float32
            )
            * score_scale
            + piece_bias[:, None, :]
        )
        query_order = first_row + jnp.arange(block_rows, dtype=jnp.int32)
        visible = key_order[None, :] <= query_order[:, None]
        piece_scores = jnp.where(visible[None], piece_scores, -jnp.inf)
        local_max = jnp.maximum(jnp.max(cache_scores, axis=-1), jnp.max(piece_scores, axis=-1))
        cache_exp = jnp.exp(cache_scores - local_max[:, :, None])
        piece_exp = jnp.exp(piece_scores - local_max[:, :, None])
        numerator = jnp.einsum(
            "hqk,khd->qhd",
            cache_exp.astype(jnp.bfloat16),
            cache_value_heads,
            preferred_element_type=jnp.float32,
        )
        numerator = numerator + jnp.einsum(
            "hqk,khd->qhd",
            piece_exp.astype(jnp.bfloat16),
            piece_value_heads,
            preferred_element_type=jnp.float32,
        )
        denominator = jnp.sum(cache_exp, axis=-1) + jnp.sum(piece_exp, axis=-1)
        return (numerator.astype(jnp.bfloat16), denominator.T, local_max.T)

    numerators, denominators, local_maxima = lax.map(block_terms, (query_blocks, block_starts))
    numerators = numerators.reshape(total_rows, local_heads, head_size)
    denominators = denominators.reshape(total_rows, local_heads)
    local_maxima = local_maxima.reshape(total_rows, local_heads)
    maxima = taken_together(local_maxima, "kv")
    factors = jnp.exp(local_maxima - maxima)
    scaled = (numerators.astype(jnp.float32) * factors[:, :, None]).astype(jnp.bfloat16)
    rounded = (
        lax.optimization_barrier(scaled)
        .astype(jnp.float32)
        .reshape(total_rows, local_heads * head_size)
    )
    denominators = denominators * factors
    own_numer = sent_and_summed(rounded.astype(jnp.bfloat16), "kv", 0)
    own_denom = sent_and_summed_2(denominators, "kv", 0)
    piece_attention = (
        own_numer.reshape(piece_count, local_heads, head_size) / own_denom[:, :, None]
    ).astype(jnp.bfloat16)
    piece_attention = piece_attention.reshape(piece_count, local_heads * head_size)
    dec_count = dec_tokens.shape[0]
    dec_span = dec_keys.shape[1]
    dec_query_heads = dec_queries.reshape(dec_count, local_heads, head_size)
    new_key_heads = dec_new_keys.reshape(dec_count, local_heads, head_size)
    new_value_heads = dec_new_values.reshape(dec_count, local_heads, head_size)
    dec_key_heads = dec_keys.reshape(dec_count, dec_span, local_heads, head_size)
    dec_value_heads = dec_values.reshape(dec_count, dec_span, local_heads, head_size)
    cached = (
        jnp.einsum(
            "bhd,bkhd->bhk", dec_query_heads, dec_key_heads, preferred_element_type=jnp.float32
        )
        * score_scale
    )
    cached = cached + dec_gates + dec_gate_now[:, :, None]
    live_slots = jnp.arange(dec_span, dtype=jnp.int32)[None, :] < dec_lengths[:, None]
    cached = jnp.where(live_slots[:, None, :], cached, -jnp.inf)
    own_score = (
        jnp.sum(dec_query_heads.astype(jnp.float32) * new_key_heads.astype(jnp.float32), axis=-1)
        * score_scale
    )
    row_top = jnp.maximum(jnp.max(cached, axis=-1), own_score)
    cached_exp = jnp.exp(cached - row_top[:, :, None])
    own_exp = jnp.exp(own_score - row_top)
    whole_sum = jnp.sum(cached_exp, axis=-1) + own_exp
    cached_weights = (cached_exp / whole_sum[:, :, None]).astype(jnp.bfloat16)
    own_weights = (own_exp / whole_sum).astype(jnp.bfloat16)
    dec_mixed = jnp.einsum(
        "bhk,bkhd->bhd", cached_weights, dec_value_heads, preferred_element_type=jnp.float32
    )
    dec_mixed = dec_mixed + own_weights.astype(jnp.float32)[:, :, None] * new_value_heads.astype(
        jnp.float32
    )
    dec_attention = dec_mixed.astype(jnp.bfloat16).reshape(dec_count, local_heads * head_size)

    def add_columns(columns_in):
        return jnp.dot(columns_in, out_weight, preferred_element_type=jnp.float32)

    column_pair = sent_together((piece_attention, dec_attention), "tp", 1, 0)
    piece_out = add_columns(column_pair[0])
    dec_out = add_columns(column_pair[1])
    return (piece_out.astype(jnp.bfloat16), dec_out.astype(jnp.bfloat16), piece_keys, piece_values)


def solution(mesh):
    return jax.shard_map(
        shards,
        mesh=mesh,
        in_specs=(
            P(("grp", "kv"), None),
            P(("grp", "kv"), None),
            P(),
            P(None, "tp"),
            P(None, "tp"),
            P(None, "tp"),
            P(None, "tp"),
            P("tp"),
            P(None, "tp"),
            P(("grp", "kv"), "tp"),
            P(("grp", "kv"), "tp"),
            P("tp", ("grp", "kv")),
            P(("grp", "kv"), None, "tp"),
            P(("grp", "kv"), None, "tp"),
            P(("grp", "kv"), "tp", None),
            P(("grp", "kv")),
        ),
        out_specs=(
            P(("grp", "kv"), "tp"),
            P(("grp", "kv"), "tp"),
            P(("grp", "kv"), "tp"),
            P(("grp", "kv"), "tp"),
        ),
        check_vma=False,
    )
```

profile of v0, /device:TPU:33, one launch (start us, length us, event | category | flops | bytes accessed | tf_op | source)
XLA Modules:
  0.0 275.1 jit_solution(3541225993187929004)
XLA Ops:
  7.3 1.7 fusion.28
  9.0 2.5 convolution_convert_fusion.3
  16.5 24.5 %all-to-all-start = ((f32[16,1,1]{2,1,0:T(1,128)}), f32[16,1,1]{2,1,0:T(1,128)S(1)}, u32[]{:S(2)}, u32[]{:S(2)}) async-start(f32[16,1,1]{2,1,0:T(1,128)} %broadcast_in_dim.35), calls=%async_computation | async-start | bytes 16384 | tf_op jit(solution)/shard_map/all_to_all | solution.py:13
  41.1 1.9 convolution_convert_fusion.1
  43.1 1.9 convolution_convert_fusion.2
  44.9 7.1 %all-to-all-done = f32[16,1,1]{2,1,0:T(1,128)S(1)} async-done(((f32[16,1,1]{2,1,0:T(1,128)}), f32[16,1,1]{2,1,0:T(1,128)S(1)}, u32[]{:S(2)}, u32[]{:S(2)}) %all-to-all-start) | async-done | bytes 96 | tf_op jit(solution)/shard_map/all_to_all | solution.py:13
  54.7 30.9 %all-gather.2.cloned.1.call-done = bf16[4096,128]{1,0:T(8,128)(2,1)} async-done(((bf16[256,128]{1,0:T(8,128)(2,1)}), bf16[4096,128]{1,0:T(8,128)(2,1)}) %all-gather.2.cloned.1.call-update) | async-done | bytes 1048592 | tf_op jit(solution)/shard_map/all_gather | solution.py:126
  85.7 76.6 %while.15 = (s32[]{:T(128)}, bf16[8,512,1,128]{3,1,2,0:T(8,128)(2,1)}, f32[8,512,1]{1,2,0:T(1,128)S(1)}, f32[8,512,1]{1,2,0:T(1,128)S(1)}, bf16[8,512,1,128]{3,1...) while((s32[]{:T(128)}, ...), condition=%wide.region_8.9_spmd.clone, body=%wide.region_3.8_spmd.clone.sunk | while | flops 1165229824 | bytes 34173624 | solution.py:177
  86.9 1.2 fusion.97
  88.1 2.2 fusion.96
  90.4 2.1 fusion.100
  92.6 1.7 fusion.98
  96.5 1.2 fusion.97
  97.7 2.2 fusion.96
  99.9 2.1 fusion.100
  102.2 1.7 fusion.98
  106.1 1.2 fusion.97
  107.3 2.2 fusion.96
  109.5 2.1 fusion.100
  111.7 1.7 fusion.98
  115.7 1.2 fusion.97
  116.8 2.2 fusion.96
  119.1 2.1 fusion.100
  121.3 1.7 fusion.98
  125.2 1.2 fusion.97
  126.4 2.2 fusion.96
  128.7 2.1 fusion.100
  130.9 1.7 fusion.98
  134.8 1.2 fusion.97
  136.0 2.2 fusion.96
  138.3 2.1 fusion.100
  140.5 1.7 fusion.98
  144.4 1.2 fusion.97
  145.6 2.2 fusion.96
  147.8 2.1 fusion.100
  150.1 1.7 fusion.98
  155.1 2.2 fusion.96
  157.4 2.1 fusion.100
  159.6 1.7 fusion.98
  162.5 19.6 %all_to_all.24 = f32[16,4096,1]{1,2,0:T(1,128)S(1)} all-to-all(f32[16,4096,1]{1,2,0:T(1,128)S(1)} %broadcast_in_dim.37), channel_id=1, replica_groups=mesh['grp'=2,'kv'=16,'tp'=8] {'kv'}, dimensions={0} | all-to-all | bytes 524288 | tf_op jit(solution)/shard_map/all_to_all | solution.py:13
  183.0 6.0 %all-to-all-start.3 = ((f32[16,256,1]{1,2,0:T(1,128)}), f32[16,256,1]{1,2,0:T(1,128)S(1)}, u32[]{:S(2)}, u32[]{:S(2)}) async-start(f32[16,256,1]{1,2,0:T(1,128)} %bitcast.104), calls=%async_computation.3 | async-start | bytes 32768 | tf_op jit(solution)/shard_map/all_to_all | solution.py:57
  189.0 2.6 fusion.31
  191.5 8.6 %all-to-all-done.3 = f32[16,256,1]{1,2,0:T(1,128)S(1)} async-done(((f32[16,256,1]{1,2,0:T(1,128)}), f32[16,256,1]{1,2,0:T(1,128)S(1)}, u32[]{:S(2)}, u32[]{:S(2)}) %all-to-all-start.3) | async-done | bytes 16416 | tf_op jit(solution)/shard_map/all_to_all | solution.py:57
  200.2 4.1 %all-to-all-start.2 = ((bf16[16,256,128]{2,1,0:T(8,128)(2,1)}), bf16[16,256,128]{2,1,0:T(8,128)(2,1)S(1)}, u32[]{:S(2)}, u32[]{:S(2)}) async-start(bf16[16,256,128]{2,1,0:T(8,128)(2,1)} %bitcast.18), calls=%async_computation.2 | async-start | bytes 2097152 | tf_op jit(solution)/shard_map/all_to_all | solution.py:51
  204.6 1.3 convolution_convert_fusion.7
  205.9 1.3 fusion.38
  209.3 28.4 %all-to-all-done.2 = bf16[16,256,128]{2,1,0:T(8,128)(2,1)S(1)} async-done(((bf16[16,256,128]{2,1,0:T(8,128)(2,1)}), bf16[16,256,128]{2,1,0:T(8,128)(2,1)S(1)}, u32[]{:S(2)}, u32[]{:S(2)}) %all-to-all-start.2) | async-done | bytes 1048608 | tf_op jit(solution)/shard_map/all_to_all | solution.py:51
  238.0 28.6 %all_gather.7 = bf16[260,1024]{1,0:T(8,128)(2,1)S(1)} all-gather(bf16[260,128]{1,0:T(8,128)(2,1)S(1)} %pad_maximum_fusion), channel_id=1, replica_groups=mesh['grp'=2,'kv'=16,'tp'=8] {'tp'}, dimensions={1}, use_global_device_ids=true | all-gather | bytes 599040 | tf_op jit(solution)/shard_map/all_gather | solution.py:63
  (161 shorter events, 29.5 us)
Async XLA Ops:
  7.2 200.2 %copy-start = (bf16[4,2048,128]{2,1,0:T(8,128)(2,1)S(1)}, bf16[4,2048,128]{2,1,0:T(8,128)(2,1)}, u32[]{:S(2)}) copy-start(bf16[4,2048,128]{2,1,0:T(8,128)(2,1)} %param.30) | copy-start | bytes 6291460
  7.2 5.0 %copy-start.5 = (bf16[256,2048]{1,0:T(8,128)(2,1)S(1)}, bf16[256,2048]{1,0:T(8,128)(2,1)}, u32[]{:S(2)}) copy-start(bf16[256,2048]{1,0:T(8,128)(2,1)} %param.18) | copy-start | bytes 3145732
  7.2 5.0 %copy-start.9 = (f32[2048]{0:T(1024)S(1)}, f32[2048]{0:T(1024)}, u32[]{:S(2)}) copy-start(f32[2048]{0:T(1024)} %param.20) | copy-start | bytes 24580
  7.2 5.0 %copy-start.13 = (bf16[2048,1]{0,1:T(2,128)(2,1)S(1)}, bf16[2048,1]{0,1:T(2,128)(2,1)}, u32[]{:S(2)}) copy-start(bf16[2048,1]{0,1:T(2,128)(2,1)} %param.24) | copy-start | bytes 12292
  7.2 78.4 %all-gather.2.cloned.1.call-start = ((), (), s32[]{:S(2)}) async-start(), calls=%async_computation.4 | async-start | bytes 1114112 | tf_op jit(solution)/shard_map/all_gather | solution.py:126
  16.5 35.5 %all-to-all-start = ((f32[16,1,1]{2,1,0:T(1,128)}), f32[16,1,1]{2,1,0:T(1,128)S(1)}, u32[]{:S(2)}, u32[]{:S(2)}) async-start(f32[16,1,1]{2,1,0:T(1,128)} %broadcast_in_dim.35), calls=%async_computation | async-start | bytes 16384 | tf_op jit(solution)/shard_map/all_to_all | solution.py:13
  41.1 44.6 %copy-start.1 = (bf16[4096,128]{1,0:T(8,128)(2,1)S(1)}, bf16[4096,128]{1,0:T(8,128)(2,1)}, u32[]{:S(2)}) copy-start(bf16[4096,128]{1,0:T(8,128)(2,1)} %param.27) | copy-start | bytes 3145732
  41.1 44.6 %copy-start.2 = (f32[1,4096]{1,0:T(1,128)S(1)}, f32[1,4096]{1,0:T(1,128)}, u32[]{:S(2)}) copy-start(f32[1,4096]{1,0:T(1,128)} %param.29) | copy-start | bytes 49156
  90.4 2.2 copy-start.11
  99.9 2.2 copy-start.11
  109.5 2.2 copy-start.11
  119.1 2.2 copy-start.11
  128.7 2.2 copy-start.11
  138.2 2.2 copy-start.11
  147.8 2.2 copy-start.11
  157.4 2.2 copy-start.11
  162.3 37.9 %copy-start.4 = (bf16[256,1,128]{2,0,1:T(8,128)(2,1)}, bf16[256,1,128]{2,0,1:T(8,128)(2,1)S(1)}, u32[]{:S(2)}) copy-start(bf16[256,1,128]{2,0,1:T(8,128)(2,1)S(1)} %get-tuple-element.330) | copy-start | bytes 196612
  162.3 37.9 %copy-start.14 = (bf16[256,1,128]{2,0,1:T(8,128)(2,1)}, bf16[256,1,128]{2,0,1:T(8,128)(2,1)S(1)}, u32[]{:S(2)}) copy-start(bf16[256,1,128]{2,0,1:T(8,128)(2,1)S(1)} %get-tuple-element.336) | copy-start | bytes 196612
  183.0 17.2 %all-to-all-start.3 = ((f32[16,256,1]{1,2,0:T(1,128)}), f32[16,256,1]{1,2,0:T(1,128)S(1)}, u32[]{:S(2)}, u32[]{:S(2)}) async-start(f32[16,256,1]{1,2,0:T(1,128)} %bitcast.104), calls=%async_computation.3 | async-start | bytes 32768 | tf_op jit(solution)/shard_map/all_to_all | solution.py:57
  189.0 15.3 %copy-start.7 = (bf16[4,2048]{1,0:T(4,128)(2,1)S(1)}, bf16[4,2048]{1,0:T(4,128)(2,1)}, u32[]{:S(2)}) copy-start(bf16[4,2048]{1,0:T(4,128)(2,1)} %param.19) | copy-start | bytes 49156
  200.2 37.5 %all-to-all-start.2 = ((bf16[16,256,128]{2,1,0:T(8,128)(2,1)}), bf16[16,256,128]{2,1,0:T(8,128)(2,1)S(1)}, u32[]{:S(2)}, u32[]{:S(2)}) async-start(bf16[16,256,128]{2,1,0:T(8,128)(2,1)} %bitcast.18), calls=%async_computation.2 | async-start | bytes 2097152 | tf_op jit(solution)/shard_map/all_to_all | solution.py:51
  204.3 3.8 %copy-start.8 = (f32[4,1,2048]{2,1,0:T(1,128)S(1)}, f32[4,1,2048]{2,1,0:T(1,128)}, u32[]{:S(2)}) copy-start(f32[4,1,2048]{2,1,0:T(1,128)} %param.32) | copy-start | bytes 98308
  204.3 3.8 %copy-start.10 = (s32[4]{0:T(128)S(1)}, s32[4]{0:T(128)}, u32[]{:S(2)}) copy-start(s32[4]{0:T(128)} %param.33) | copy-start | bytes 52
  204.3 4.2 %copy-start.3 = (bf16[4,2048,128]{2,1,0:T(8,128)(2,1)S(1)}, bf16[4,2048,128]{2,1,0:T(8,128)(2,1)}, u32[]{:S(2)}) copy-start(bf16[4,2048,128]{2,1,0:T(8,128)(2,1)} %param.31) | copy-start | bytes 6291460
  207.4 1.6 copy-start.12
  237.7 28.9 %copy-start.6 = (bf16[1024,256]{1,0:T(8,128)(2,1)S(1)}, bf16[1024,256]{1,0:T(8,128)(2,1)}, u32[]{:S(2)}) copy-start(bf16[1024,256]{1,0:T(8,128)(2,1)} %param.26) | copy-start | bytes 1572868
Sparse Core Ops, SparseCore 0:
  11.7 73.9 all-gather.1
where the time goes:
time: 276 us; the launch traced here: 275 us
  waiting for transfers between devices  75.2 us (27%)
  matrix products  61.2 us (22%)
  blocking collectives  48.2 us (17%)
  starting transfers between devices  34.7 us (13%)
  other arithmetic  29.6 us (11%)
  between operations  17.6 us (6%)
  local copies, waits for them, and re-layouts  8.3 us (3%)
    all_gather x1, waiting for transfers between devices, shards(): all_queries = lax.all_gather(piece_queries, 'kv', axis=0, tiled=True)  30.9 us
    all_gather x1, blocking collectives, sent_together(): lax.all_gather(both, axis, axis=dim, tiled=True)  28.6 us
    all_to_all x1, waiting for transfers between devices, sent_and_summed(): lax.all_to_all(cut_along(shard, dim, devices), axis, 0, 0, tiled=True)  28.4 us
    all_to_all x1, starting transfers between devices, from_everyone(): lax.all_to_all(jnp.broadcast_to(shard[None], (devices, *shard.shape)), ax...  24.5 us
    all_to_all x1, blocking collectives, from_everyone(): lax.all_to_all(jnp.broadcast_to(shard[None], (devices, *shard.shape)), ax...  19.6 us
    dot_general x8, matrix products, block_terms(): jnp.einsum('qhd,khd->hqk', query_block, cache_key_heads, preferred_elemen...  18 us
    reduce_sum x16, other arithmetic, block_terms(): denominator = jnp.sum(cache_exp, axis=-1) + jnp.sum(piece_exp, axis=-1)  17.4 us
    dot_general x8, matrix products, block_terms(): jnp.einsum('hqk,khd->qhd', cache_exp.astype(jnp.bfloat16), cache_value_he...  13.8 us
  transfers between devices with their start and end apart: 4, of which 4 were waited for; matrix products, arithmetic and copies ran while one was open for 6% of the time, Pallas kernels for 0%

commit v1 on v0

v1 whole, which is shorter than its diff:
```python
import functools
import math

import jax
import jax.numpy as jnp
from jax import lax
from jax.experimental import pallas as pl
from jax.experimental.pallas import tpu as pltpu
from jax.sharding import PartitionSpec as P

norm_eps = 1e-05
bf16 = jnp.bfloat16
f32 = jnp.float32
MESH = pl.DeviceIdType.MESH
NEG = -1e30
LANES = 128
KEY_CHUNK = 2048


def dot(a, b):
    return jnp.dot(a, b, preferred_element_type=f32)


def three_parts(x):
    high = x.astype(bf16)
    rest = x - high.astype(f32)
    middle = rest.astype(bf16)
    low = (rest - middle.astype(f32)).astype(bf16)
    return high, middle, low


def row_max(x, rows=64):
    n = x.shape[0]
    if n > rows:
        x = jnp.max(x.reshape(n // rows, rows, x.shape[1]), axis=0)
    return jnp.max(x, axis=0, keepdims=True)


def kernel(
    tok_hbm,
    dtok_ref,
    gain_ref,
    wq_hbm,
    wk_hbm,
    wv_hbm,
    fw_ref,
    fb_ref,
    ow_hbm,
    ck_hbm,
    cv_hbm,
    cg_ref,
    dk_hbm,
    dv_hbm,
    dg_ref,
    dl_ref,
    po_ref,
    do_ref,
    pk_ref,
    pv_ref,
    tok,
    wq,
    wk,
    wv,
    ow,
    cv,
    dk,
    dv,
    normed,
    kaug,
    v_t,
    ones_rows,
    qbuf,
    acc_in,
    ml_in,
    acc_out,
    ml_out,
    unit_acc,
    unit_ml,
    own_acc,
    own_ml,
    totals,
    att,
    datt,
    local_sem,
    q_send,
    q_recv,
    acc_send,
    acc_recv,
    ml_send,
    ml_recv,
    tot_send,
    tot_recv,
    att_send,
    att_recv,
    datt_send,
    datt_recv,
    *,
    chains,
):
    n = lax.axis_size("kv")
    heads = lax.axis_size("tp")
    me = lax.axis_index("kv")
    my_tp = lax.axis_index("tp")
    right = lax.rem(me + 1, n)
    left = lax.rem(me + n - 1, n)
    piece, width = tok.shape
    half = piece // 2
    depth = wq.shape[1]
    cache = cv.shape[0]
    decs, span = dk.shape[0], dk.shape[1]
    length = n // chains
    scale = depth ** (-0.5)
    root = depth**0.5
    c2 = scale * math.log2(math.e)

    def load(i, src, dst):
        return pltpu.make_async_copy(src, dst, local_sem.at[i])

    loads = [
        load(0, tok_hbm, tok),
        load(1, wq_hbm, wq),
        load(2, wk_hbm, wk),
        load(3, wv_hbm, wv),
        load(4, cv_hbm, cv),
        load(5, ck_hbm, kaug.at[pl.ds(0, cache), pl.ds(0, depth)]),
        load(6, dk_hbm, dk),
        load(7, dv_hbm, dv),
        load(8, ow_hbm, ow),
    ]
    barrier = pltpu.get_barrier_semaphore()
    for d in range(1, n):
        pl.semaphore_signal(
            barrier, inc=1, device_id={"kv": lax.rem(me + d, n)}, device_id_type=MESH
        )
    for d in range(1, heads):
        pl.semaphore_signal(
            barrier, inc=1, device_id={"tp": lax.rem(my_tp + d, heads)}, device_id_type=MESH
        )
    for c in loads:
        c.start()

    def total_copy(d):
        return pltpu.make_async_remote_copy(
            src_ref=totals.at[0],
            dst_ref=totals.at[d],
            send_sem=tot_send.at[d],
            recv_sem=tot_recv.at[d],
            device_id={"kv": lax.rem(me + d, n)},
            device_id_type=MESH,
        )

    def q_copy(src, dst, side, target):
        return pltpu.make_async_remote_copy(
            src_ref=qbuf.at[src, side],
            dst_ref=qbuf.at[dst, side],
            send_sem=q_send.at[dst, side],
            recv_sem=q_recv.at[dst, side],
            device_id={"kv": target},
            device_id_type=MESH,
        )

    def acc_copies(src, dst, side, target):
        return (
            pltpu.make_async_remote_copy(
                src_ref=acc_out.at[src, side],
                dst_ref=acc_in.at[dst, side],
                send_sem=acc_send.at[src, side],
                recv_sem=acc_recv.at[dst, side],
                device_id={"kv": target},
                device_id_type=MESH,
            ),
            pltpu.make_async_remote_copy(
                src_ref=ml_out.at[src, side],
                dst_ref=ml_in.at[dst, side],
                send_sem=ml_send.at[src, side],
                recv_sem=ml_recv.at[dst, side],
                device_id={"kv": target},
                device_id_type=MESH,
            ),
        )

    def att_copy(d, src_slot, dst_slot):
        return pltpu.make_async_remote_copy(
            src_ref=att.at[src_slot],
            dst_ref=att.at[dst_slot],
            send_sem=att_send.at[d],
            recv_sem=att_recv.at[d],
            device_id={"tp": lax.rem(my_tp + d, heads)},
            device_id_type=MESH,
        )

    def datt_copy(d, src_slot, dst_slot):
        return pltpu.make_async_remote_copy(
            src_ref=datt.at[src_slot],
            dst_ref=datt.at[dst_slot],
            send_sem=datt_send.at[d],
            recv_sem=datt_recv.at[d],
            device_id={"tp": lax.rem(my_tp + d, heads)},
            device_id_type=MESH,
        )

    gain = gain_ref[...]
    rows_at_once = 64

    def norm_rows(x):
        x = x.astype(f32)
        factor = lax.rsqrt(jnp.mean(x * x, axis=-1, keepdims=True) + norm_eps)
        return (x * factor * gain).astype(bf16)

    loads[0].wait()
    for r in range(0, piece, rows_at_once):
        normed[r : r + rows_at_once, :] = norm_rows(tok[r : r + rows_at_once, :])
    drows = norm_rows(dtok_ref[...])
    normed[piece:, :] = jnp.concatenate(
        [drows, jnp.zeros((normed.shape[0] - piece - decs, width), bf16)], axis=0
    )
    loads[1].wait()
    queries = dot(normed[...], wq[...]).astype(bf16)
    q_t = queries[:piece, :].T
    for side in range(2):
        qbuf[0, side] = q_t[:, side * half : (side + 1) * half]
    gate_in = dot(normed[...], fw_ref[...])[:, 0:1] + fb_ref[...]
    log_gates = jnp.minimum(gate_in, 0.0) - jnp.log1p(jnp.exp(-jnp.abs(gate_in)))
    piece_gates = log_gates[:piece]
    lane = lax.broadcasted_iota(jnp.int32, (piece, LANES), 1)
    hi, mid, lo = three_parts(piece_gates)
    zero = jnp.zeros((), f32)

    def columns(a, b, c, rows):
        at = lax.broadcasted_iota(jnp.int32, (rows, LANES), 1)
        out = jnp.where(at == 0, a.astype(f32), zero)
        out = jnp.where(at == 1, b.astype(f32), out)
        out = jnp.where(at == 2, c.astype(f32), out)
        return out.astype(bf16)

    below = (
        lax.broadcasted_iota(jnp.int32, (piece, piece), 1)
        <= lax.broadcasted_iota(jnp.int32, (piece, piece), 0)
    ).astype(f32)
    running = dot(below.astype(bf16), columns(hi, mid, lo, piece))
    running = running[:, 0:1] + running[:, 1:2] + running[:, 2:3]
    totals[0] = jnp.broadcast_to(running[piece - 1 : piece, :], (8, LANES))

    pl.semaphore_wait(barrier, n - 1 + heads - 1)
    for side, target in ((0, right), (1, left)):
        q_copy(0, 1, side, target).start()
    for d in range(1, n):
        total_copy(d).start()
    for c in range(1, chains):
        o = 1 + c * length
        q_copy(0, o, 0, lax.rem(me + o, n)).start()
        q_copy(0, o, 1, lax.rem(me - o + n, n)).start()

    loads[2].wait()
    key_rows = dot(normed[...], wk[...]).astype(bf16)
    pk_ref[...] = key_rows[:piece]
    kaug[cache:, :depth] = key_rows[:piece]
    loads[3].wait()
    value_rows = dot(normed[...], wv[...]).astype(bf16)
    pv_ref[...] = value_rows[:piece]
    v_t[:depth, cache:] = value_rows[:piece].T
    v_t[depth:, :] = jnp.ones((v_t.shape[0] - depth, v_t.shape[1]), bf16)
    kaug[cache:, depth:] = columns(*three_parts(-running * root), piece)
    at_row = lax.broadcasted_iota(jnp.int32, (LANES, 2 * piece), 0)
    ones_rows[...] = jnp.where(at_row < 3, 1.0, 0.0)[:, :piece].astype(bf16)
    for r in range(0, cache, 512):
        gates = jnp.maximum(cg_ref[:, r : r + 512], NEG) * root
        a, b, c = three_parts(gates)
        at = lax.broadcasted_iota(jnp.int32, (LANES, 512), 0)
        rows = jnp.where(at == 0, a.astype(f32), zero)
        rows = jnp.where(at == 1, b.astype(f32), rows)
        rows = jnp.where(at == 2, c.astype(f32), rows)
        kaug[r : r + 512, depth:] = rows.astype(bf16).T
    loads[4].wait()
    for r in range(0, cache, 512):
        v_t[:depth, r : r + 512] = cv[r : r + 512, :].T
    loads[5].wait()

    loads[6].wait()
    dec_q = queries[piece:, :]
    dec_k = key_rows[piece:, :]
    dec_v = value_rows[piece:, :]
    scores = []
    for b in range(decs):
        s = lax.dot_general(
            dec_q, dk[b], (((1,), (1,)), ((), ())), preferred_element_type=f32
        )
        scores.append(s[b : b + 1])
    cached = jnp.concatenate(scores, axis=0) * scale + dg_ref[...] + log_gates[piece : piece + decs]
    slot = lax.broadcasted_iota(jnp.int32, (decs, span), 1)
    cached = jnp.where(slot < dl_ref[...], cached, -jnp.inf)
    own_score = (
        jnp.sum(dec_q.astype(f32) * dec_k.astype(f32), axis=-1, keepdims=True)[:decs] * scale
    )
    top = jnp.maximum(jnp.max(cached, axis=-1, keepdims=True), own_score)
    cached_exp = jnp.exp(cached - top)
    own_exp = jnp.exp(own_score - top)
    whole = jnp.sum(cached_exp, axis=-1, keepdims=True) + own_exp
    weights = (cached_exp / whole).astype(bf16)
    own_weight = (own_exp / whole).astype(bf16).astype(f32)
    weights = jnp.concatenate(
        [weights, jnp.zeros((dec_q.shape[0] - decs, span), bf16)], axis=0
    )
    loads[7].wait()
    mixed = [dot(weights, dv[b])[b : b + 1] for b in range(decs)]
    mixed = jnp.concatenate(mixed, axis=0) + own_weight * dec_v[:decs].astype(f32)
    datt[0] = jnp.concatenate(
        [mixed, jnp.zeros((dec_q.shape[0] - decs, depth), f32)], axis=0
    ).astype(bf16)
    for d in range(1, heads):
        datt_copy(d, 0, d).start()

    chunks = [(cache, cache + piece)] + [
        (k, k + KEY_CHUNK) for k in range(0, cache, KEY_CHUNK)
    ]
    lane_row = lax.broadcasted_iota(jnp.int32, (1, piece), 1)

    def local_terms(o, offset):
        block_a = lax.rem(me - o + n, n)
        block_b = lax.rem(me + o, n)
        slot_o = lax.rem(o, n)
        q_block = jnp.concatenate([qbuf[slot_o, 0], qbuf[slot_o, 1]], axis=1)
        q_block = jnp.concatenate([q_block, ones_rows[...]], axis=0)
        query_order = jnp.where(lane_row < half, block_a, block_b) * piece + lane_row
        s = dot(kaug[chunks[0][0] : chunks[0][1], :], q_block)
        terms = []
        for i, (k0, k1) in enumerate(chunks):
            if i == 0:
                key_order = me * piece + lax.broadcasted_iota(jnp.int32, (piece, 1), 0)
                s = jnp.where(key_order <= query_order, s, NEG)
            top_i = row_max(s)
            if i + 1 < len(chunks):
                s_next = dot(kaug[chunks[i + 1][0] : chunks[i + 1][1], :], q_block)
            weights_i = jnp.exp2((s - top_i) * c2).astype(bf16)
            sums = dot(v_t[:, k0:k1], weights_i)
            terms.append((sums, top_i - offset * root if i == 0 else top_i))
            s = s_next
        top_all = functools.reduce(jnp.maximum, [t for _, t in terms])
        total = None
        for sums, t in terms:
            part = sums * jnp.exp2((t - top_all) * c2)
            total = part if total is None else total + part
        return total[:depth], top_all, total[depth : depth + 1]

    def ml_rows(m, l):
        return jnp.concatenate([m, l, jnp.zeros((6, m.shape[1]), f32)], axis=0)

    def merge(acc_a, m_a, l_a, acc_b, m_b, l_b):
        m = jnp.maximum(m_a, m_b)
        f_a = jnp.exp2((m_a - m) * c2)
        f_b = jnp.exp2((m_b - m) * c2)
        return acc_a * f_a + acc_b * f_b, m, l_a * f_a + l_b * f_b

    for d in range(1, n):
        total_copy(d).wait_recv()
    offset = jnp.zeros((1, LANES), f32)
    for d in range(1, n):
        offset = offset + jnp.where(d <= me, totals[d][0:1, :], 0.0)
    offset = jnp.concatenate([offset] * (piece // LANES), axis=1)

    skew = 2 if chains > 1 else 0
    paired = length - skew if chains > 1 else 0

    def order(u):
        if chains == 1:
            return jnp.where(u == 0, n, u)
        k = u - 1 - skew
        middle = jnp.where(
            lax.rem(k, 2) == 0, 1 + skew + k // 2, 1 + length + k // 2
        )
        o = jnp.where(u < 1 + skew, u, jnp.where(k < 2 * paired, middle, u))
        return jnp.where(u == 0, n, o)

    def unit(u, carry):
        o = order(u)
        starts = lax.rem(o, length) == 1
        ends = lax.rem(o, length) == 0

        @pl.when(o < n)
        def _():
            for side in range(2):
                q_copy(0, o, side, right).wait_recv()

        @pl.when(jnp.logical_and(jnp.logical_not(ends), o < n - 1))
        def _():
            for side, target in ((0, right), (1, left)):
                q_copy(o, o + 1, side, target).start()

        acc, m, l = local_terms(o, offset)
        unit_acc[...] = acc
        unit_ml[...] = ml_rows(m, l)

        @pl.when(o == n)
        def _():
            own_acc[...] = unit_acc[...]
            own_ml[...] = unit_ml[...]

        @pl.when(o < n)
        def _():
            @pl.when(starts)
            def _():
                for side in range(2):
                    acc_in[o, side] = jnp.zeros((depth, half), bf16)
                    ml_in[o, side] = jnp.where(
                        lax.broadcasted_iota(jnp.int32, (8, half), 0) == 0, NEG, 0.0
                    )

            @pl.when(jnp.logical_not(starts))
            def _():
                for side in range(2):
                    for c in acc_copies(0, o, side, right):
                        c.wait_recv()

            for side in range(2):
                at = slice(side * half, (side + 1) * half)
                ml = ml_in[o, side]
                a, mm, ll = merge(
                    unit_acc[:, at],
                    unit_ml[0:1, at],
                    unit_ml[1:2, at],
                    acc_in[o, side].astype(f32),
                    ml[0:1],
                    ml[1:2],
                )
                acc_out[o, side] = a.astype(bf16)
                ml_out[o, side] = ml_rows(mm, ll)
            goes = jnp.where(ends, o, 1)
            dst = jnp.where(ends, n + o // length, o + 1)
            for c in acc_copies(o, dst, 0, lax.rem(me + jnp.where(ends, n - goes, 1), n)):
                c.start()
            for c in acc_copies(o, dst, 1, lax.rem(me + jnp.where(ends, goes, n - 1), n)):
                c.start()

        return carry

    lax.fori_loop(0, n, unit, 0)

    halves = []
    for side in range(2):
        at = slice(side * half, (side + 1) * half)
        state = (own_acc[:, at], own_ml[0:1, at], own_ml[1:2, at])
        for slot_i in [n + c for c in range(1, chains)] + [n]:
            for c in acc_copies(0, slot_i, side, right):
                c.wait_recv()
            ml = ml_in[slot_i, side]
            state = merge(*state, acc_in[slot_i, side].astype(f32), ml[0:1], ml[1:2])
        halves.append((state[0] / state[2]).astype(bf16))
    att[0] = jnp.concatenate(halves, axis=1).T
    for d in range(1, heads):
        att_copy(d, 0, d).start()

    def weight_of(d):
        head = lax.rem(my_tp - d + heads, heads)
        return ow[pl.ds(pl.multiple_of(head * depth, depth), depth), :]

    loads[8].wait()
    dec_sum = dot(datt[0], weight_of(0))
    for d in range(1, heads):
        datt_copy(d, 0, d).wait_recv()
        dec_sum = dec_sum + dot(datt[d], weight_of(d))
    do_ref[...] = dec_sum[:decs].astype(bf16)
    out = dot(att[0], weight_of(0))
    for d in range(1, heads):
        att_copy(d, 0, d).wait_recv()
        out = out + dot(att[d], weight_of(d))
    po_ref[...] = out.astype(bf16)

    for d in range(1, n):
        total_copy(d).wait_send()
    for d in range(1, heads):
        att_copy(d, 0, d).wait_send()
        datt_copy(d, 0, d).wait_send()

    def sent(o, carry):
        for side in range(2):
            q_copy(0, o, side, right).wait_send()
            for c in acc_copies(o, n, side, right):
                c.wait_send()
        return carry

    lax.fori_loop(1, n, sent, 0)


def shards(
    piece_tokens,
    dec_tokens,
    norm_gain,
    query_weight,
    key_weight,
    value_weight,
    forget_weight,
    forget_bias,
    out_weight,
    cache_keys,
    cache_values,
    cache_gates,
    dec_keys,
    dec_values,
    dec_gates,
    dec_lengths,
):
    n = lax.axis_size("kv")
    heads = lax.axis_size("tp")
    piece, width = piece_tokens.shape
    decs, span = dec_tokens.shape[0], dec_keys.shape[1]
    depth = query_weight.shape[1]
    cache = cache_keys.shape[0]
    out_columns = out_weight.shape[1]
    half = piece // 2
    chains = 2
    rows = piece + 16
    vmem = pl.BlockSpec(memory_space=pltpu.VMEM)
    hbm = pl.BlockSpec(memory_space=pl.ANY)
    dma = pltpu.SemaphoreType.DMA
    slots = n + chains
    gate_weight = jnp.concatenate(
        [forget_weight, jnp.zeros((width, LANES - forget_weight.shape[1]), bf16)], axis=1
    )
    return pl.pallas_call(
        functools.partial(kernel, chains=chains),
        out_shape=(
            jax.ShapeDtypeStruct((piece, out_columns), bf16),
            jax.ShapeDtypeStruct((decs, out_columns), bf16),
            jax.ShapeDtypeStruct((piece, depth), bf16),
            jax.ShapeDtypeStruct((piece, depth), bf16),
        ),
        in_specs=[hbm, vmem, vmem, hbm, hbm, hbm, vmem, vmem, hbm, hbm, hbm, vmem, hbm, hbm, vmem, vmem],
        out_specs=(vmem, vmem, vmem, vmem),
        scratch_shapes=[
            pltpu.VMEM((piece, width), bf16),
            pltpu.VMEM((width, depth), bf16),
            pltpu.VMEM((width, depth), bf16),
            pltpu.VMEM((width, depth), bf16),
            pltpu.VMEM(out_weight.shape, bf16),
            pltpu.VMEM((cache, depth), bf16),
            pltpu.VMEM(dec_keys.shape, bf16),
            pltpu.VMEM(dec_values.shape, bf16),
            pltpu.VMEM((rows, width), bf16),
            pltpu.VMEM((cache + piece, depth + LANES), bf16),
            pltpu.VMEM((depth + 16, cache + piece), bf16),
            pltpu.VMEM((LANES, piece), bf16),
            pltpu.VMEM((n, 2, depth, half), bf16),
            pltpu.VMEM((slots, 2, depth, half), bf16),
            pltpu.VMEM((slots, 2, 8, half), f32),
            pltpu.VMEM((n, 2, depth, half), bf16),
            pltpu.VMEM((n, 2, 8, half), f32),
            pltpu.VMEM((depth, piece), f32),
            pltpu.VMEM((8, piece), f32),
            pltpu.VMEM((depth, piece), f32),
            pltpu.VMEM((8, piece), f32),
            pltpu.VMEM((n, 8, LANES), f32),
            pltpu.VMEM((heads, piece, depth), bf16),
            pltpu.VMEM((heads, 16, depth), bf16),
            dma((9,)),
            dma((n, 2)),
            dma((n, 2)),
            dma((n, 2)),
            dma((slots, 2)),
            dma((n, 2)),
            dma((slots, 2)),
            dma((n,)),
            dma((n,)),
            dma((heads,)),
            dma((heads,)),
            dma((heads,)),
            dma((heads,)),
        ],
        compiler_params=pltpu.CompilerParams(
            collective_id=0, has_side_effects=True, vmem_limit_bytes=60 * 2**20
        ),
    )(
        piece_tokens,
        dec_tokens,
        norm_gain.reshape(1, width),
        query_weight,
        key_weight,
        value_weight,
        gate_weight,
        forget_bias.reshape(1, 1),
        out_weight,
        cache_keys,
        cache_values,
        cache_gates,
        dec_keys,
        dec_values,
        dec_gates.reshape(decs, span),
        dec_lengths.reshape(decs, 1),
    )


def solution(mesh):
    return jax.shard_map(
        shards,
        mesh=mesh,
        in_specs=(
            P(("grp", "kv"), None),
            P(("grp", "kv"), None),
            P(),
            P(None, "tp"),
            P(None, "tp"),
            P(None, "tp"),
            P(None, "tp"),
            P("tp"),
            P(None, "tp"),
            P(("grp", "kv"), "tp"),
            P(("grp", "kv"), "tp"),
            P("tp", ("grp", "kv")),
            P(("grp", "kv"), None, "tp"),
            P(("grp", "kv"), None, "tp"),
            P(("grp", "kv"), "tp", None),
            P(("grp", "kv")),
        ),
        out_specs=(
            P(("grp", "kv"), "tp"),
            P(("grp", "kv"), "tp"),
            P(("grp", "kv"), "tp"),
            P(("grp", "kv"), "tp"),
        ),
        check_vma=False,
    )
```

time: 276 us -> 109 us (0.39)
  Pallas kernels: 0 us -> 96.9 us
  waiting for transfers between devices: 75.2 us -> 0 us
  matrix products: 61.2 us -> 0 us
  blocking collectives: 48.2 us -> 0 us
  starting transfers between devices: 34.7 us -> 0 us
  other arithmetic: 29.6 us -> 0 us
  between operations: 17.6 us -> 1.3 us
    pallas_call x0 -> x1, Pallas kernels: none -> 96.9 us  [shards(): pl.pallas_call(functools.partial(kernel, chains=chains), out_shape=(jax.S...]
    dot_general x44 -> x0, matrix products: 61.2 us -> none  [the longest x8 18 us: block_terms(): jnp.einsum('qhd,khd->hqk', query_block, cache_key_heads, preferred_elemen...]
    all_to_all x3 -> x0, waiting for transfers between devices: 44.2 us -> none  [the longest x1 28.4 us: sent_and_summed(): lax.all_to_all(cut_along(shard, dim, devices), axis, 0, 0, tiled=True)]
    all_to_all x3 -> x0, starting transfers between devices: 34.6 us -> none  [the longest x1 24.5 us: from_everyone(): lax.all_to_all(jnp.broadcast_to(shard[None], (devices, *shard.shape)), ax...]
    all_gather x1 -> x0, waiting for transfers between devices: 30.9 us -> none  [shards(): all_queries = lax.all_gather(piece_queries, 'kv', axis=0, tiled=True)]
    all_gather x1 -> x0, blocking collectives: 28.6 us -> none  [sent_together(): lax.all_gather(both, axis, axis=dim, tiled=True)]
    reduce_sum x21 -> x0, other arithmetic: 19.6 us -> none  [the longest x16 17.4 us: block_terms(): denominator = jnp.sum(cache_exp, axis=-1) + jnp.sum(piece_exp, axis=-1)]
    all_to_all x1 -> x0, blocking collectives: 19.6 us -> none  [from_everyone(): lax.all_to_all(jnp.broadcast_to(shard[None], (devices, *shard.shape)), ax...]
  transfers between devices with their start and end apart: 4 -> 0, of which waited for: 4 -> 0; matrix products, arithmetic and copies ran while one was open for 6% -> 0% of each run, Pallas kernels for 0% -> 0%
where the time goes in v1:
time: 109 us
  Pallas kernels  96.9 us (89%)
  local copies, waits for them, and re-layouts  10.4 us (10%)
  between operations  1.3 us (1%)
    pallas_call x1, Pallas kernels, shards(): pl.pallas_call(functools.partial(kernel, chains=chains), out_shape=(jax.S...  96.9 us
    unnamed x6, local copies, waits for them, and re-layouts  8.16 us

profile of v1, /device:TPU:33, one launch (start us, length us, event | category | flops | bytes accessed | tf_op | source)
XLA Modules:
  0.0 108.6 jit_solution(13068793692367109404)
XLA Ops:
  0.6 1.0 copy.20
  1.6 0.9 concatenate.3.fw_ref
  2.5 1.4 %copy.24 = f32[4,1,2048]{2,0,1:T(4,128)} copy(f32[4,1,2048]{2,1,0:T(1,128)} %param.30) | data formatting | bytes 65536
  3.9 1.3 %copy.21.dl_ref = s32[4,1]{1,0:T(4,128)} copy(s32[4,1]{0,1:T(1,128)} %bitcast.9) | data formatting | bytes 32 | tf_op jit(solution)/shard_map/reshape | solution.py:587
  5.9 96.9 %shard_map.183 = (bf16[256,256]{1,0:T(8,128)(2,1)}, bf16[4,256]{1,0:T(4,128)(2,1)}, bf16[256,128]{1,0:T(8,128)(2,1)}, bf16[256,128]{1,0:T(8,128)(2,1)}) custom-call(bf16[256,2048]{1,0:T(8,128)(2,1)} %tok_hbm.1, bf16[4,2048]{1,0:T(4,128)(2,1)} %dtok_ref.1, f32[1,2048]{1,0:T(1,128)} %bitcast.8, bf16[2048,128]{1,0:T(8,128)(2,1)} %wq_hbm.1, ...), custom_call_target="tpu_custom_call" | custom-call | tf_op jit(solution)/shard_map/pallas_call | solution.py:519
  102.8 1.6 %copy.30 = bf16[256,256]{1,0:T(8,128)(2,1)} copy(bf16[256,256]{1,0:T(8,128)(2,1)} %get-tuple-element.8) | data formatting | bytes 262144
  104.4 1.3 %copy.31 = bf16[4,256]{1,0:T(4,128)(2,1)} copy(bf16[4,256]{1,0:T(4,128)(2,1)} %get-tuple-element.9) | data formatting | bytes 4096
  105.6 1.5 %copy.32 = bf16[256,128]{1,0:T(8,128)(2,1)} copy(bf16[256,128]{1,0:T(8,128)(2,1)} %get-tuple-element.10) | data formatting | bytes 131072
  107.1 1.5 %copy.33 = bf16[256,128]{1,0:T(8,128)(2,1)} copy(bf16[256,128]{1,0:T(8,128)(2,1)} %get-tuple-element.11) | data formatting | bytes 131072

commit v2 on v1

--- a/solution.py
+++ b/solution.py
@@ -81,6 +81,8 @@
     totals,
     att,
     datt,
+    dec_rows,
+    dec_gate,
     local_sem,
     q_send,
     q_recv,
@@ -127,6 +129,8 @@
         load(7, dv_hbm, dv),
         load(8, ow_hbm, ow),
     ]
+    loads[0].start()
+    loads[1].start()
     barrier = pltpu.get_barrier_semaphore()
     for d in range(1, n):
         pl.semaphore_signal(
@@ -136,13 +140,11 @@
         pl.semaphore_signal(
             barrier, inc=1, device_id={"tp": lax.rem(my_tp + d, heads)}, device_id_type=MESH
         )
-    for c in loads:
-        c.start()
 
     def total_copy(d):
         return pltpu.make_async_remote_copy(
-            src_ref=totals.at[0],
-            dst_ref=totals.at[d],
+            src_ref=totals.at[0, pl.ds(0, 1)],
+            dst_ref=totals.at[d, pl.ds(0, 1)],
             send_sem=tot_send.at[d],
             recv_sem=tot_recv.at[d],
             device_id={"kv": lax.rem(me + d, n)},
@@ -170,8 +172,8 @@
                 device_id_type=MESH,
             ),
             pltpu.make_async_remote_copy(
-                src_ref=ml_out.at[src, side],
-                dst_ref=ml_in.at[dst, side],
+                src_ref=ml_out.at[src, side, pl.ds(0, 2)],
+                dst_ref=ml_in.at[dst, side, pl.ds(0, 2)],
                 send_sem=ml_send.at[src, side],
                 recv_sem=ml_recv.at[dst, side],
                 device_id={"kv": target},
@@ -208,6 +210,8 @@
         return (x * factor * gain).astype(bf16)
 
     loads[0].wait()
+    for c in loads[2:]:
+        c.start()
     for r in range(0, piece, rows_at_once):
         normed[r : r + rows_at_once, :] = norm_rows(tok[r : r + rows_at_once, :])
     drows = norm_rows(dtok_ref[...])
@@ -219,7 +223,13 @@
     q_t = queries[:piece, :].T
     for side in range(2):
         qbuf[0, side] = q_t[:, side * half : (side + 1) * half]
-    gate_in = dot(normed[...], fw_ref[...])[:, 0:1] + fb_ref[...]
+    gate_rows = jnp.broadcast_to(fw_ref[...], (LANES, width))
+    gate_in = (
+        lax.dot_general(
+            normed[...], gate_rows, (((1,), (1,)), ((), ())), preferred_element_type=f32
+        )[:, 0:1]
+        + fb_ref[0]
+    )
     log_gates = jnp.minimum(gate_in, 0.0) - jnp.log1p(jnp.exp(-jnp.abs(gate_in)))
     piece_gates = log_gates[:piece]
     lane = lax.broadcasted_iota(jnp.int32, (piece, LANES), 1)
@@ -276,39 +286,49 @@
         v_t[:depth, r : r + 512] = cv[r : r + 512, :].T
     loads[5].wait()
 
-    loads[6].wait()
-    dec_q = queries[piece:, :]
-    dec_k = key_rows[piece:, :]
-    dec_v = value_rows[piece:, :]
-    scores = []
-    for b in range(decs):
-        s = lax.dot_general(
-            dec_q, dk[b], (((1,), (1,)), ((), ())), preferred_element_type=f32
-        )
-        scores.append(s[b : b + 1])
-    cached = jnp.concatenate(scores, axis=0) * scale + dg_ref[...] + log_gates[piece : piece + decs]
-    slot = lax.broadcasted_iota(jnp.int32, (decs, span), 1)
-    cached = jnp.where(slot < dl_ref[...], cached, -jnp.inf)
-    own_score = (
-        jnp.sum(dec_q.astype(f32) * dec_k.astype(f32), axis=-1, keepdims=True)[:decs] * scale
-    )
-    top = jnp.maximum(jnp.max(cached, axis=-1, keepdims=True), own_score)
-    cached_exp = jnp.exp(cached - top)
-    own_exp = jnp.exp(own_score - top)
-    whole = jnp.sum(cached_exp, axis=-1, keepdims=True) + own_exp
-    weights = (cached_exp / whole).astype(bf16)
-    own_weight = (own_exp / whole).astype(bf16).astype(f32)
-    weights = jnp.concatenate(
-        [weights, jnp.zeros((dec_q.shape[0] - decs, span), bf16)], axis=0
-    )
-    loads[7].wait()
-    mixed = [dot(weights, dv[b])[b : b + 1] for b in range(decs)]
-    mixed = jnp.concatenate(mixed, axis=0) + own_weight * dec_v[:decs].astype(f32)
-    datt[0] = jnp.concatenate(
-        [mixed, jnp.zeros((dec_q.shape[0] - decs, depth), f32)], axis=0
-    ).astype(bf16)
-    for d in range(1, heads):
-        datt_copy(d, 0, d).start()
+    dec_rows[0] = queries[piece:, :]
+    dec_rows[1] = key_rows[piece:, :]
+    dec_rows[2] = value_rows[piece:, :]
+    dec_gate[...] = jnp.broadcast_to(log_gates[piece:, :], dec_gate.shape)
+
+    def decode():
+        loads[6].wait()
+        dec_q = dec_rows[0]
+        dec_k = dec_rows[1]
+        dec_v = dec_rows[2]
+        scores = []
+        for b in range(decs):
+            s = lax.dot_general(
+                dec_q, dk[b], (((1,), (1,)), ((), ())), preferred_element_type=f32
+            )
+            scores.append(s[b : b + 1])
+        gates = jnp.concatenate([dg_ref[b] for b in range(decs)], axis=0)
+        cached = jnp.concatenate(scores, axis=0) * scale + gates + dec_gate[0:decs, 0:1]
+        slot = lax.broadcasted_iota(jnp.int32, (1, span), 1)
+        live = jnp.concatenate(
+            [jnp.where(slot < dl_ref[b], 1.0, 0.0) for b in range(decs)], axis=0
+        )
+        cached = jnp.where(live > 0.5, cached, -jnp.inf)
+        own_score = (
+            jnp.sum(dec_q.astype(f32) * dec_k.astype(f32), axis=-1, keepdims=True)[:decs] * scale
+        )
+        top = jnp.maximum(jnp.max(cached, axis=-1, keepdims=True), own_score)
+        cached_exp = jnp.exp(cached - top)
+        own_exp = jnp.exp(own_score - top)
+        whole = jnp.sum(cached_exp, axis=-1, keepdims=True) + own_exp
+        weights = (cached_exp / whole).astype(bf16)
+        own_weight = (own_exp / whole).astype(bf16).astype(f32)
+        weights = jnp.concatenate(
+            [weights, jnp.zeros((dec_q.shape[0] - decs, span), bf16)], axis=0
+        )
+        loads[7].wait()
+        mixed = [dot(weights, dv[b])[b : b + 1] for b in range(decs)]
+        mixed = jnp.concatenate(mixed, axis=0) + own_weight * dec_v[:decs].astype(f32)
+        datt[0] = jnp.concatenate(
+            [mixed, jnp.zeros((dec_q.shape[0] - decs, depth), f32)], axis=0
+        ).astype(bf16)
+        for d in range(1, heads):
+            datt_copy(d, 0, d).start()
 
     chunks = [(cache, cache + piece)] + [
         (k, k + KEY_CHUNK) for k in range(0, cache, KEY_CHUNK)
@@ -363,13 +383,13 @@
 
     def order(u):
         if chains == 1:
-            return jnp.where(u == 0, n, u)
+            return jnp.where(u == 0, 1, jnp.where(u == 1, n, u))
         k = u - 1 - skew
         middle = jnp.where(
             lax.rem(k, 2) == 0, 1 + skew + k // 2, 1 + length + k // 2
         )
         o = jnp.where(u < 1 + skew, u, jnp.where(k < 2 * paired, middle, u))
-        return jnp.where(u == 0, n, o)
+        return jnp.where(u == 0, 1, jnp.where(u == 1, n, o))
 
     def unit(u, carry):
         o = order(u)
@@ -385,6 +405,10 @@
         def _():
             for side, target in ((0, right), (1, left)):
                 q_copy(o, o + 1, side, target).start()
+
+        @pl.when(u == 2)
+        def _():
+            decode()
 
         acc, m, l = local_terms(o, offset)
         unit_acc[...] = acc
@@ -479,6 +503,11 @@
         return carry
 
     lax.fori_loop(1, n, sent, 0)
+
+
+def hand_over(*refs):
+    for src, dst in zip(refs[:4], refs[4:]):
+        dst[...] = src[...]
 
 
 def shards(
@@ -513,10 +542,8 @@
     hbm = pl.BlockSpec(memory_space=pl.ANY)
     dma = pltpu.SemaphoreType.DMA
     slots = n + chains
-    gate_weight = jnp.concatenate(
-        [forget_weight, jnp.zeros((width, LANES - forget_weight.shape[1]), bf16)], axis=1
-    )
-    return pl.pallas_call(
+    smem = pl.BlockSpec(memory_space=pltpu.SMEM)
+    results = pl.pallas_call(
         functools.partial(kernel, chains=chains),
         out_shape=(
             jax.ShapeDtypeStruct((piece, out_columns), bf16),
@@ -524,7 +551,7 @@
             jax.ShapeDtypeStruct((piece, depth), bf16),
             jax.ShapeDtypeStruct((piece, depth), bf16),
         ),
-        in_specs=[hbm, vmem, vmem, hbm, hbm, hbm, vmem, vmem, hbm, hbm, hbm, vmem, hbm, hbm, vmem, vmem],
+        in_specs=[hbm, vmem, vmem, hbm, hbm, hbm, vmem, smem, hbm, hbm, hbm, vmem, hbm, hbm, vmem, smem],
         out_specs=(vmem, vmem, vmem, vmem),
         scratch_shapes=[
             pltpu.VMEM((piece, width), bf16),
@@ -551,6 +578,8 @@
             pltpu.VMEM((n, 8, LANES), f32),
             pltpu.VMEM((heads, piece, depth), bf16),
             pltpu.VMEM((heads, 16, depth), bf16),
+            pltpu.VMEM((3, 16, depth), bf16),
+            pltpu.VMEM((16, LANES), f32),
             dma((9,)),
             dma((n, 2)),
             dma((n, 2)),
@@ -575,17 +604,23 @@
         query_weight,
         key_weight,
         value_weight,
-        gate_weight,
-        forget_bias.reshape(1, 1),
+        forget_weight.reshape(1, width),
+        forget_bias,
         out_weight,
         cache_keys,
         cache_values,
         cache_gates,
         dec_keys,
         dec_values,
-        dec_gates.reshape(decs, span),
-        dec_lengths.reshape(decs, 1),
+        dec_gates,
+        dec_lengths,
     )
+    return pl.pallas_call(
+        hand_over,
+        out_shape=tuple(jax.ShapeDtypeStruct(r.shape, r.dtype) for r in results),
+        in_specs=[vmem] * 4,
+        out_specs=(vmem,) * 4,
+    )(*results)
 
 
 def solution(mesh):

time: 109 us -> 98.8 us (0.906)
  local copies, waits for them, and re-layouts: 10.4 us -> 0 us
    unnamed x6 -> x0, local copies, waits for them, and re-layouts: 8.16 us -> none
    pallas_call x0 -> x1, Pallas kernels: none -> 1.65 us  [shards(): pl.pallas_call(hand_over, out_shape=tuple((jax.ShapeDtypeStruct(r.shape,...]
    reshape x1 -> x0, local copies, waits for them, and re-layouts: 1.31 us -> none  [shards(): dec_lengths.reshape(decs, 1)]
    pallas_call x1, Pallas kernels: 96.9 us -> 95.7 us  [shards(): pl.pallas_call(functools.partial(kernel, chains=chains), out_shape=(jax.S...]
where the time goes in v2:
time: 98.8 us; the launch traced here: 98.6 us
  Pallas kernels  97.3 us (98%)
  between operations  1.29 us (1%)
    pallas_call x1, Pallas kernels, shards(): pl.pallas_call(functools.partial(kernel, chains=chains), out_shape=(jax.S...  95.7 us

profile of v2, /device:TPU:33, one launch (start us, length us, event | category | flops | bytes accessed | tf_op | source)
XLA Modules:
  0.0 98.6 jit_solution(8382674429200569107)
XLA Ops:
  1.3 95.7 %shard_map.183 = (bf16[256,256]{1,0:T(8,128)(2,1)}, bf16[4,256]{1,0:T(4,128)(2,1)}, bf16[256,128]{1,0:T(8,128)(2,1)}, bf16[256,128]{1,0:T(8,128)(2,1)}) custom-call(bf16[256,2048]{1,0:T(8,128)(2,1)} %tok_hbm.1, bf16[4,2048]{1,0:T(4,128)(2,1)} %dtok_ref.1, f32[1,2048]{1,0:T(1,128)} %bitcast.2, bf16[2048,128]{1,0:T(8,128)(2,1)} %wq_hbm.1, ...), custom_call_target="tpu_custom_call" | custom-call | tf_op jit(solution)/shard_map/pallas_call | solution.py:546
  96.9 1.6 %shard_map.184 = (bf16[256,256]{1,0:T(8,128)(2,1)}, bf16[4,256]{1,0:T(4,128)(2,1)}, bf16[256,128]{1,0:T(8,128)(2,1)}, bf16[256,128]{1,0:T(8,128)(2,1)}) custom-call(bf16[256,256]{1,0:T(8,128)(2,1)} %get-tuple-element.8.refs_0_, bf16[4,256]{1,0:T(4,128)(2,1)} %get-tuple-element.9.refs_1_, bf16[256,128]{1,0:T(8,128)(2,1)} %get-tuple-element.10.refs_2_, ...), custom_call_target="tpu_custom_call" | custom-call | tf_op jit(solution)/shard_map/pallas_call | solution.py:618

commit v3 on v2

--- a/solution.py
+++ b/solution.py
@@ -96,8 +96,6 @@
     att_recv,
     datt_send,
     datt_recv,
-    *,
-    chains,
 ):
     n = lax.axis_size("kv")
     heads = lax.axis_size("tp")
@@ -110,7 +108,7 @@
     depth = wq.shape[1]
     cache = cv.shape[0]
     decs, span = dk.shape[0], dk.shape[1]
-    length = n // chains
+    split = n // 2
     scale = depth ** (-0.5)
     root = depth**0.5
     c2 = scale * math.log2(math.e)
@@ -256,10 +254,9 @@
         q_copy(0, 1, side, target).start()
     for d in range(1, n):
         total_copy(d).start()
-    for c in range(1, chains):
-        o = 1 + c * length
-        q_copy(0, o, 0, lax.rem(me + o, n)).start()
-        q_copy(0, o, 1, lax.rem(me - o + n, n)).start()
+    second = split + 1
+    q_copy(0, second, 0, lax.rem(me + second, n)).start()
+    q_copy(0, second, 1, lax.rem(me - second + n, n)).start()
 
     loads[2].wait()
     key_rows = dot(normed[...], wk[...]).astype(bf16)
@@ -335,32 +332,38 @@
     ]
     lane_row = lax.broadcasted_iota(jnp.int32, (1, piece), 1)
 
-    def local_terms(o, offset):
-        block_a = lax.rem(me - o + n, n)
-        block_b = lax.rem(me + o, n)
-        slot_o = lax.rem(o, n)
-        q_block = jnp.concatenate([qbuf[slot_o, 0], qbuf[slot_o, 1]], axis=1)
-        q_block = jnp.concatenate([q_block, ones_rows[...]], axis=0)
-        query_order = jnp.where(lane_row < half, block_a, block_b) * piece + lane_row
-        s = dot(kaug[chunks[0][0] : chunks[0][1], :], q_block)
-        terms = []
-        for i, (k0, k1) in enumerate(chunks):
-            if i == 0:
+    def local_terms(offsets, shift):
+        steps = []
+        for which, o in enumerate(offsets):
+            block_a = lax.rem(me - o + n, n)
+            block_b = lax.rem(me + o, n)
+            slot_o = lax.rem(o, n)
+            q_block = jnp.concatenate([qbuf[slot_o, 0], qbuf[slot_o, 1]], axis=1)
+            q_block = jnp.concatenate([q_block, ones_rows[...]], axis=0)
+            query_order = jnp.where(lane_row < half, block_a, block_b) * piece + lane_row
+            steps += [(which, q_block, query_order, k0, k1) for k0, k1 in chunks]
+        terms = [[] for _ in offsets]
+        s = dot(kaug[steps[0][3] : steps[0][4], :], steps[0][1])
+        for i, (which, q_block, query_order, k0, k1) in enumerate(steps):
+            if k0 == cache:
                 key_order = me * piece + lax.broadcasted_iota(jnp.int32, (piece, 1), 0)
                 s = jnp.where(key_order <= query_order, s, NEG)
             top_i = row_max(s)
-            if i + 1 < len(chunks):
-                s_next = dot(kaug[chunks[i + 1][0] : chunks[i + 1][1], :], q_block)
+            if i + 1 < len(steps):
+                s_next = dot(kaug[steps[i + 1][3] : steps[i + 1][4], :], steps[i + 1][1])
             weights_i = jnp.exp2((s - top_i) * c2).astype(bf16)
             sums = dot(v_t[:, k0:k1], weights_i)
-            terms.append((sums, top_i - offset * root if i == 0 else top_i))
+            terms[which].append((sums, top_i - shift * root if k0 == cache else top_i))
             s = s_next
-        top_all = functools.reduce(jnp.maximum, [t for _, t in terms])
-        total = None
-        for sums, t in terms:
-            part = sums * jnp.exp2((t - top_all) * c2)
-            total = part if total is None else total + part
-        return total[:depth], top_all, total[depth : depth + 1]
+        results = []
+        for mine in terms:
+            top_all = functools.reduce(jnp.maximum, [t for _, t in mine])
+            total = None
+            for sums, t in mine:
+                part = sums * jnp.exp2((t - top_all) * c2)
+                total = part if total is None else total + part
+            results.append((total[:depth], top_all, total[depth : depth + 1]))
+        return results
 
     def ml_rows(m, l):
         return jnp.concatenate([m, l, jnp.zeros((6, m.shape[1]), f32)], axis=0)
@@ -378,92 +381,94 @@
         offset = offset + jnp.where(d <= me, totals[d][0:1, :], 0.0)
     offset = jnp.concatenate([offset] * (piece // LANES), axis=1)
 
-    skew = 2 if chains > 1 else 0
-    paired = length - skew if chains > 1 else 0
-
-    def order(u):
-        if chains == 1:
-            return jnp.where(u == 0, 1, jnp.where(u == 1, n, u))
-        k = u - 1 - skew
-        middle = jnp.where(
-            lax.rem(k, 2) == 0, 1 + skew + k // 2, 1 + length + k // 2
-        )
-        o = jnp.where(u < 1 + skew, u, jnp.where(k < 2 * paired, middle, u))
-        return jnp.where(u == 0, 1, jnp.where(u == 1, n, o))
-
-    def unit(u, carry):
-        o = order(u)
-        starts = lax.rem(o, length) == 1
-        ends = lax.rem(o, length) == 0
-
-        @pl.when(o < n)
+    def arrived(o):
+        for side in range(2):
+            q_copy(0, o, side, right).wait_recv()
+
+    def forward(o):
+        for side, target in ((0, right), (1, left)):
+            q_copy(o, o + 1, side, target).start()
+
+    def settle(which, o, starts, ends):
+        @pl.when(starts)
         def _():
             for side in range(2):
-                q_copy(0, o, side, right).wait_recv()
-
-        @pl.when(jnp.logical_and(jnp.logical_not(ends), o < n - 1))
+                acc_in[o, side] = jnp.zeros((depth, half), bf16)
+                ml_in[o, side] = jnp.where(
+                    lax.broadcasted_iota(jnp.int32, (8, half), 0) == 0, NEG, 0.0
+                )
+
+        @pl.when(jnp.logical_not(starts))
         def _():
-            for side, target in ((0, right), (1, left)):
-                q_copy(o, o + 1, side, target).start()
-
-        @pl.when(u == 2)
+            for side in range(2):
+                for c in acc_copies(0, o, side, right):
+                    c.wait_recv()
+
+        away = jnp.where(ends, o, n - 1)
+        dst = jnp.where(ends, n + 1, o + 1)
+        targets = (lax.rem(me + n - jnp.where(ends, o, n - 1), n), lax.rem(me + away, n))
+        for side in range(2):
+            at = slice(side * half, (side + 1) * half)
+            ml = ml_in[o, side]
+            a, mm, ll = merge(
+                unit_acc[which, :, at],
+                unit_ml[which, 0:1, at],
+                unit_ml[which, 1:2, at],
+                acc_in[o, side].astype(f32),
+                ml[0:1],
+                ml[1:2],
+            )
+            acc_out[o, side] = a.astype(bf16)
+            ml_out[o, side] = ml_rows(mm, ll)
+        for side in range(2):
+            for c in acc_copies(o, dst, side, targets[side]):
+                c.start()
+
+    def pair(it, carry):
+        first = it + 1
+        other = jnp.where(it == 0, n, split + it)
+        arrived(first)
+
+        @pl.when(first < split)
+        def _():
+            forward(first)
+
+        @pl.when(it == 1)
         def _():
             decode()
 
-        acc, m, l = local_terms(o, offset)
-        unit_acc[...] = acc
-        unit_ml[...] = ml_rows(m, l)
-
-        @pl.when(o == n)
+        @pl.when(it > 0)
         def _():
-            own_acc[...] = unit_acc[...]
-            own_ml[...] = unit_ml[...]
-
-        @pl.when(o < n)
+            arrived(other)
+
+            @pl.when(other < n - 1)
+            def _():
+                forward(other)
+
+        for which, (acc, m, l) in enumerate(local_terms((first, other), offset)):
+            unit_acc[which] = acc
+            unit_ml[which] = ml_rows(m, l)
+
+        settle(0, first, it == 0, first == split)
+
+        @pl.when(it == 0)
         def _():
-            @pl.when(starts)
-            def _():
-                for side in range(2):
-                    acc_in[o, side] = jnp.zeros((depth, half), bf16)
-                    ml_in[o, side] = jnp.where(
-                        lax.broadcasted_iota(jnp.int32, (8, half), 0) == 0, NEG, 0.0
-                    )
-
-            @pl.when(jnp.logical_not(starts))
-            def _():
-                for side in range(2):
-                    for c in acc_copies(0, o, side, right):
-                        c.wait_recv()
-
-            for side in range(2):
-                at = slice(side * half, (side + 1) * half)
-                ml = ml_in[o, side]
-                a, mm, ll = merge(
-                    unit_acc[:, at],
-                    unit_ml[0:1, at],
-                    unit_ml[1:2, at],
-                    acc_in[o, side].astype(f32),
-                    ml[0:1],
-                    ml[1:2],
-                )
-                acc_out[o, side] = a.astype(bf16)
-                ml_out[o, side] = ml_rows(mm, ll)
-            goes = jnp.where(ends, o, 1)
-            dst = jnp.where(ends, n + o // length, o + 1)
-            for c in acc_copies(o, dst, 0, lax.rem(me + jnp.where(ends, n - goes, 1), n)):
-                c.start()
-            for c in acc_copies(o, dst, 1, lax.rem(me + jnp.where(ends, goes, n - 1), n)):
-                c.start()
+            own_acc[...] = unit_acc[1]
+            own_ml[...] = unit_ml[1]
+
+        @pl.when(it > 0)
+        def _():
+            settle(1, other, it == 1, other == n)
 
         return carry
 
-    lax.fori_loop(0, n, unit, 0)
+    lax.fori_loop(0, split, pair, 0)
 
     halves = []
     for side in range(2):
         at = slice(side * half, (side + 1) * half)
         state = (own_acc[:, at], own_ml[0:1, at], own_ml[1:2, at])
-        for slot_i in [n + c for c in range(1, chains)] + [n]:
+        for slot_i in (n + 1, n):
             for c in acc_copies(0, slot_i, side, right):
                 c.wait_recv()
             ml = ml_in[slot_i, side]
@@ -536,15 +541,14 @@
     cache = cache_keys.shape[0]
     out_columns = out_weight.shape[1]
     half = piece // 2
-    chains = 2
     rows = piece + 16
     vmem = pl.BlockSpec(memory_space=pltpu.VMEM)
     hbm = pl.BlockSpec(memory_space=pl.ANY)
     dma = pltpu.SemaphoreType.DMA
-    slots = n + chains
+    slots = n + 2
     smem = pl.BlockSpec(memory_space=pltpu.SMEM)
     results = pl.pallas_call(
-        functools.partial(kernel, chains=chains),
+        kernel,
         out_shape=(
             jax.ShapeDtypeStruct((piece, out_columns), bf16),
             jax.ShapeDtypeStruct((decs, out_columns), bf16),
@@ -571,8 +575,8 @@
             pltpu.VMEM((slots, 2, 8, half), f32),
             pltpu.VMEM((n, 2, depth, half), bf16),
             pltpu.VMEM((n, 2, 8, half), f32),
-            pltpu.VMEM((depth, piece), f32),
-            pltpu.VMEM((8, piece), f32),
+            pltpu.VMEM((2, depth, piece), f32),
+            pltpu.VMEM((2, 8, piece), f32),
             pltpu.VMEM((depth, piece), f32),
             pltpu.VMEM((8, piece), f32),
             pltpu.VMEM((n, 8, LANES), f32),

time: 98.8 us -> 93.2 us (0.943)
  Pallas kernels: 97.3 us -> 91 us
    pallas_call x1, Pallas kernels: 95.7 us -> 89.4 us  [shards(): pl.pallas_call(kernel, out_shape=(jax.ShapeDtypeStruct((piece, out_column...]
where the time goes in v3:
time: 93.2 us; the launch traced here: 92.3 us
  Pallas kernels  91 us (98%)
  between operations  1.29 us (1%)
    pallas_call x1, Pallas kernels, shards(): pl.pallas_call(kernel, out_shape=(jax.ShapeDtypeStruct((piece, out_column...  89.4 us

profile of v3, /device:TPU:33, one launch (start us, length us, event | category | flops | bytes accessed | tf_op | source)
XLA Modules:
  0.0 92.3 jit_solution(15080504459355084556)
XLA Ops:
  1.3 89.4 %shard_map.183 = (bf16[256,256]{1,0:T(8,128)(2,1)}, bf16[4,256]{1,0:T(4,128)(2,1)}, bf16[256,128]{1,0:T(8,128)(2,1)}, bf16[256,128]{1,0:T(8,128)(2,1)}) custom-call(bf16[256,2048]{1,0:T(8,128)(2,1)} %tok_hbm.1, bf16[4,2048]{1,0:T(4,128)(2,1)} %dtok_ref.1, f32[1,2048]{1,0:T(1,128)} %bitcast.2, bf16[2048,128]{1,0:T(8,128)(2,1)} %wq_hbm.1, ...), custom_call_target="tpu_custom_call" | custom-call | tf_op jit(solution)/shard_map/pallas_call | solution.py:550
  90.6 1.6 %shard_map.184 = (bf16[256,256]{1,0:T(8,128)(2,1)}, bf16[4,256]{1,0:T(4,128)(2,1)}, bf16[256,128]{1,0:T(8,128)(2,1)}, bf16[256,128]{1,0:T(8,128)(2,1)}) custom-call(bf16[256,256]{1,0:T(8,128)(2,1)} %get-tuple-element.8.refs_0_, bf16[4,256]{1,0:T(4,128)(2,1)} %get-tuple-element.9.refs_1_, bf16[256,128]{1,0:T(8,128)(2,1)} %get-tuple-element.10.refs_2_, ...), custom_call_target="tpu_custom_call" | custom-call | tf_op jit(solution)/shard_map/pallas_call | solution.py:622
